TPU v7x, 32 devices: a whole 2x2x4 slice. The times are simulated.
32 devices in a mesh: ep: 8 (over z, x), tp: 4 (over y, core).
Axes of the slice: x: 2, y: 2, z: 4, core: 2. Of those that a mesh axis runs over, the one named last changes fastest.
Arguments:
- hidden_in: bfloat16 [256, 4096], P('ep'), may hold values from -6 to 6
- norm_gain: float32 [4096], replicated, may hold values from 0.1 to 1.9
- group_ids: int32 [256], P('ep'), may hold values from 0 to 1, as said below
- inner_ids: int32 [256, 4], P('ep'), may hold values from 0 to 7, as said below
- group_prob: float32 [256], P('ep'), may hold values from 0.25 to 1
- expert_prob: float32 [256, 4], P('ep'), may hold values from 0.1 to 1
- w_gate: bfloat16 [16, 4096, 1024], P('ep', None, 'tp'), may hold values from -0.09375 to 0.09375
- w_up: bfloat16 [16, 4096, 1024], P('ep', None, 'tp'), may hold values from -0.09375 to 0.09375
- w_down: bfloat16 [16, 1024, 4096], P('ep', None, 'tp'), may hold values from -0.1875 to 0.1875
Outputs:
- moe_out: bfloat16 [256, 4096], P('ep', 'tp')
Inputs may be any that keep to these rules, and one draw needn't show every extreme that they name: `group_ids`: among the 32 tokens of one index of ep no group is named by more than 16 tokens; one group is named by exactly 16 of them, and all of these name one common expert of it. `inner_ids`: each row names 4 different experts of the token's group.
All inputs are finite; a program needn't handle non-finite values.
Results may differ from a plain program's by a relative error of at most 0.0069.
Values may be sent and summed in bfloat16 or wider, within the bound.
A program may use at most 64 MiB of HBM per device.

v0:
```python
import functools

import jax
import jax.numpy as jnp
from jax import lax
from jax.experimental import pallas as pl
from jax.experimental.pallas import tpu as pltpu
from jax.sharding import PartitionSpec as P

EPG = 8
EPS = 1e-06
CORES = 2
LANES = 128
CHUNKS = 2
MESH = pl.DeviceIdType.MESH


def rem(value, count):
    return lax.rem(value + count, count)


def moe_kernel(
    ep_count, tp_count,
    hid_hbm, gain_hbm, grp_hbm, inner_hbm, gprob_hbm, eprob_hbm, wg_hbm, wu_hbm, wd_hbm,
    out_ref,
    hid_ref, gain_ref, grp_ref, inner_ref, gprob_ref, eprob_ref,
    wg, wu, wd, rows_out, rows_own, rows_in, acts, parts, back,
    i_sem, w_sem, step_send, a_recv, s_recv, q_recv, b_recv, r_recv, h_recv, hr_recv, o_recv,
):
    experts, depth, hidden = wg.shape
    ranks = EPG // experts
    groups = ep_count // ranks
    ys = tp_count // CORES
    tokens = hid_ref.shape[0]
    cap = tokens // 2
    feats = depth // tp_count
    side = depth // CORES
    cols = wd.shape[2]

    me_ep, me_tp = lax.axis_index("ep"), lax.axis_index("tp")
    g, p = lax.div(me_ep, ranks), lax.rem(me_ep, ranks)
    y, c = lax.div(me_tp, CORES), lax.rem(me_tp, CORES)
    sib = 1 - c

    barrier = pltpu.get_barrier_semaphore()
    partners = 0

    def shift(rank, d, sign):
        return rem(lax.div(rank, 2) + sign * (d // 2), ranks // 2) * 2 + rem(
            lax.rem(rank, 2) + sign * (d % 2), 2
        )

    def to(d):
        return shift(p, d, 1)

    def of(d):
        return shift(p, d, -1)

    def twin(dy=0):
        return (lax.rem(y + dy, ys) if dy else y) * CORES + sib

    def greet(ep, tp):
        pl.semaphore_signal(
            barrier, inc=1, device_id={"ep": ep, "tp": tp}, device_id_type=MESH
        )

    for j in range(1, groups):
        greet(rem(g - j, groups) * ranks + p, twin())
        partners += 1
    for d in range(ranks):
        for dy in range(ys):
            greet(g * ranks + to(d), twin(dy))
            partners += 1

    fetched = []
    for k, (src, dst) in enumerate((
        (hid_hbm, hid_ref), (gain_hbm, gain_ref), (grp_hbm, grp_ref), (inner_hbm, inner_ref),
        (gprob_hbm, gprob_ref), (eprob_hbm, eprob_ref),
    )):
        load = pltpu.make_async_copy(src, dst, i_sem.at[k])
        load.start()
        fetched.append(load)
    for load in fetched:
        load.wait()
    loads = []
    for k, (src, dst) in enumerate(((wg_hbm, wg), (wu_hbm, wu), (wd_hbm, wd))):
        load = pltpu.make_async_copy(src, dst, w_sem.at[k])
        load.start()
        loads.append(load)

    r0 = lax.broadcasted_iota(jnp.int32, (tokens, tokens), 0)
    r1 = lax.broadcasted_iota(jnp.int32, (tokens, tokens), 1)
    grow = jnp.broadcast_to(grp_ref[...], (tokens, tokens))
    gcol = jnp.sum(jnp.where(r0 == r1, grow, 0), axis=1, keepdims=True)
    same = gcol == grow
    rank_row = jnp.sum(jnp.where(same & (r0 < r1), 1, 0), axis=0, keepdims=True)
    rank_col = jnp.sum(jnp.where(same & (r1 < r0), 1, 0), axis=1, keepdims=True)

    def slot(group, rank):
        rel = g - group
        return jnp.where(rel < 0, rel + groups, rel) * cap + rank

    slots = groups * cap
    pick = (
        lax.broadcasted_iota(jnp.int32, (slots, tokens), 0) == slot(grp_ref[...], rank_row)
    ).astype(jnp.bfloat16)

    line = lax.broadcasted_iota(jnp.int32, (LANES, tokens), 0)
    inner, eprob, prob = inner_ref[...], eprob_ref[...], gprob_ref[...]
    weight = jnp.zeros((LANES, tokens), jnp.float32)
    for k in range(inner.shape[0]):
        hit = lax.rem(line, EPG) == inner[k : k + 1, :]
        weight += jnp.where(hit, prob * eprob[k : k + 1, :], 0.0)
    high = weight.astype(jnp.bfloat16).astype(jnp.float32)
    mid = (weight - high).astype(jnp.bfloat16).astype(jnp.float32)
    low = weight - high - mid
    part = lax.div(line, EPG)
    weight = jnp.where(
        part == 0, high, jnp.where(part == 1, mid, jnp.where(part == 2, low, 0.0))
    ).astype(jnp.bfloat16)
    wdat = lax.dot_general(
        pick, weight, (((1,), (1,)), ((), ())), preferred_element_type=jnp.float32
    ).astype(jnp.bfloat16)

    x = hid_ref[...].astype(jnp.float32)
    scale = lax.rsqrt(jnp.mean(x * x, axis=-1, keepdims=True) + EPS)

    def normed(cut):
        return (
            hid_ref[:, cut].astype(jnp.float32) * scale * gain_ref[:, cut]
        ).astype(jnp.bfloat16)

    if groups > 1:
        mine = pl.ds(pl.multiple_of(me_tp * feats, LANES), feats)
        data = jnp.dot(
            pick[cap:], normed(mine), preferred_element_type=jnp.float32
        ).astype(jnp.bfloat16)
        for j in range(1, groups):
            rows_out[j - 1, :, :feats] = data[(j - 1) * cap : j * cap]
            rows_out[j - 1, :, feats:] = wdat[j * cap : (j + 1) * cap]

    with jax.named_scope("barrier"):
        pl.semaphore_wait(barrier, partners)
    pending = {}

    def bulk(size):
        return wg.at[0, : size // (hidden * 2)]

    def send(src, dst, ssem, rsem, ep, tp, key):
        pltpu.make_async_remote_copy(
            src_ref=src, dst_ref=dst, send_sem=ssem, recv_sem=rsem,
            device_id={"ep": ep, "tp": tp}, device_id_type=MESH,
        ).start()
        size = 2
        for extent in src.shape:
            size *= extent
        pending[key] = (ssem, pending.get(key, (ssem, 0))[1] + size)

    def wait_of(dst, sem):
        return pltpu.make_async_remote_copy(
            src_ref=dst, dst_ref=dst, send_sem=sem, recv_sem=sem,
            device_id={"ep": me_ep, "tp": me_tp}, device_id_type=MESH,
        )

    def landed(dst, sem):
        wait_of(dst, sem).wait_recv()

    def lines(rank):
        start = rank * cap
        return pl.ds(start if isinstance(rank, int) else pl.multiple_of(start, cap), cap)

    def piece(j, core, yy, rank):
        return rows_in.at[j, core, yy, lines(rank)]

    def own(core, rank):
        return rows_own.at[core, lines(rank)]

    for j in range(1, groups):
        send(rows_out.at[j - 1], piece(j, c, y, p), step_send.at[j],
             a_recv.at[j - 1], rem(g - j, groups) * ranks + p, twin(), j)

    for core in range(CORES):
        cut = slice(core * side, (core + 1) * side)
        rows_own[core, lines(p), :side] = jnp.dot(
            pick[:cap], normed(cut), preferred_element_type=jnp.float32
        ).astype(jnp.bfloat16)
        rows_own[core, lines(p), side:] = wdat[:cap]

    near = sorted(range(1, ranks), key=lambda d: -(d // 2 + d % 2))
    hops = [
        (d, dy) for dy in reversed(range(ys)) for d in near + [0] if d or dy
    ]

    for d in near:
        send(own(c, p), own(c, p), step_send.at[0], s_recv.at[d - 1], g * ranks + to(d), twin(), 0)

    def relay_own():
        for d in near:
            got = own(sib, of(d))
            landed(got, s_recv.at[d - 1])
            send(got, got, step_send.at[0], q_recv.at[0], me_ep, twin(), 0)

    def spread(j):
        held = piece(j, sib, y, p)
        bare = held.at[:, :feats]
        for i, (d, dy) in enumerate(hops):
            part = bare if dy else held
            send(part, part, step_send.at[j], b_recv.at[j - 1, i], g * ranks + to(d), twin(dy), j)
        send(bare, bare, step_send.at[j], r_recv.at[j - 1, 0], me_ep, twin(), j)

    def chunks(j):
        count = 1 if j == 0 else CHUNKS
        size = ranks * cap // count
        return [slice(k * size, (k + 1) * size) for k in range(count)]

    def expand(j):
        gates = [jnp.zeros((ranks * cap, hidden), jnp.float32) for _ in range(experts)]
        ups = [jnp.zeros((ranks * cap, hidden), jnp.float32) for _ in range(experts)]

        def multiply(load, ks):
            lhs = load(slice(None))
            for e in range(experts):
                gates[e] += jnp.dot(lhs, wg[e, ks, :], preferred_element_type=jnp.float32)
                ups[e] += jnp.dot(lhs, wu[e, ks, :], preferred_element_type=jnp.float32)

        def finish(load, ks, wrow):
            lanes = lax.broadcasted_iota(jnp.int32, wrow.shape, 1)
            scales = [
                jnp.sum(
                    jnp.where(lax.rem(lanes, EPG) == p * experts + e, wrow, 0.0),
                    axis=1, keepdims=True,
                ) for e in range(experts)
            ]
            multiply(load, ks)
            for k, rows in enumerate(chunks(j)):
                for e in range(experts):
                    gate, up = gates[e][rows], ups[e][rows]
                    act = gate / (1.0 + jnp.exp(-gate)) * up * scales[e][rows]
                    acts[j, c, y, rows, e * hidden : (e + 1) * hidden] = act.astype(jnp.bfloat16)
                held = acts.at[j, c, y, rows]
                for dy in range(1, ys):
                    send(held, held, step_send.at[j], h_recv.at[j, k, dy - 1], me_ep, twin(dy), j)
                send(held, held, step_send.at[j], hr_recv.at[j, k, 0], me_ep, twin(), j)

        if j == 0:
            def half(core):
                return (
                    lambda rows: rows_own[core, rows, :side],
                    pl.ds(pl.multiple_of(core * side, side), side),
                )

            multiply(*half(sib))
            landed(rows_own.at[c, : (ranks - 1) * cap], q_recv.at[0])
            finish(*half(c), rows_own[sib, :, side:].astype(jnp.float32))
            return

        def quarter(core, dy):
            yy = rem(y - dy, ys)
            return (
                lambda rows: rows_in[j, core, yy, rows, :feats],
                pl.ds(pl.multiple_of((yy * CORES + core) * feats, feats), feats),
            )

        for dy in reversed(range(ys)):
            for i, (d, hop) in enumerate(hops):
                if hop == dy:
                    got = piece(j, c, rem(y - dy, ys), of(d))
                    landed(got.at[:, :feats] if dy else got, b_recv.at[j - 1, i])
                    got = got.at[:, :feats]
                    send(got, got, step_send.at[j], r_recv.at[j - 1, 1 + dy], me_ep, twin(), j)
            if dy == 0:
                landed(piece(j, c, y, p).at[:, :feats], r_recv.at[j - 1, 0])
            multiply(*quarter(c, dy))
        rows_in[j, c, y, lines(p), feats:] = rows_in[j, sib, y, lines(p), feats:]
        wrow = rows_in[j, c, y, :, feats:].astype(jnp.float32)
        for dy in reversed(range(ys)):
            landed(bulk((ranks - (dy == 0)) * cap * feats * 2), r_recv.at[j - 1, 1 + dy])
            if dy:
                multiply(*quarter(sib, dy))
            else:
                finish(*quarter(sib, dy), wrow)

    def collect(j):
        landed(parts.at[j, : (ranks - 1 if j == 0 else ranks) * cap], o_recv.at[j])

    def contract(j):
        def multiply(core, dy, rows, total):
            yy = rem(y - dy, ys)
            ks = pl.ds(pl.multiple_of((yy * CORES + core) * hidden, hidden), hidden)
            for e in range(experts):
                total += jnp.dot(
                    acts[j, core, yy, rows, e * hidden : (e + 1) * hidden],
                    wd[e, ks, :], preferred_element_type=jnp.float32,
                )
            return total

        cuts = chunks(j)
        whole = multiply(c, 0, slice(None), jnp.zeros((ranks * cap, cols), jnp.float32))
        for k in range(len(cuts)):
            landed(acts.at[j, sib, y, cuts[k]], hr_recv.at[j, k, 0])
        whole = multiply(sib, 0, slice(None), whole)

        def relay(k):
            for dy in range(1, ys):
                got = acts.at[j, sib, rem(y - dy, ys), cuts[k]]
                landed(got, h_recv.at[j, k, dy - 1])
                send(got, got, step_send.at[j], hr_recv.at[j, k, dy], me_ep, twin(), j)

        relay(0)
        for k, rows in enumerate(cuts):
            if k:
                collect(j - 1)
            total = whole[rows]
            for dy in range(1, ys):
                total = multiply(sib, dy, rows, total)
            if k + 1 < len(cuts):
                relay(k + 1)
            for dy in range(1, ys):
                landed(acts.at[j, c, rem(y - dy, ys), rows], hr_recv.at[j, k, dy])
                total = multiply(c, dy, rows, total)
            parts[j, rows] = total.astype(jnp.bfloat16)
            if j == 0:
                for d in near:
                    send(parts.at[0, lines(to(d))], back.at[0, p], step_send.at[0], o_recv.at[0],
                         g * ranks + to(d), me_tp, 0)
                back[0, p] = parts[0, lines(p), :]
                continue
            for r in range(rows.start // cap, rows.stop // cap):
                send(parts.at[j, lines(r)], back.at[j, p], step_send.at[j], o_recv.at[j],
                     lax.rem(g + j, groups) * ranks + r, me_tp, j)

    for j in range(groups):
        if j + 1 < groups:
            with jax.named_scope(f"a_wait{j+1}"):
                landed(piece(j + 1, sib, y, p), a_recv.at[j])
            spread(j + 1)
        if j == 0:
            with jax.named_scope("relay0"):
                relay_own()
            loads[0].wait()
            loads[1].wait()
        with jax.named_scope(f"expand{j}"):
            expand(j)
        if j:
            if j == 1:
                loads[2].wait()
            with jax.named_scope(f"contract{j-1}"):
                contract(j - 1)
    if groups == 1:
        loads[2].wait()
    with jax.named_scope("contractL"):
        contract(groups - 1)

    with jax.named_scope("back1"):
        collect(groups - 1)
    with jax.named_scope("final"):
        spot = lax.broadcasted_iota(jnp.int32, (tokens, ranks * slots), 1)
        spot = lax.div(spot, ranks * cap) * cap + lax.rem(spot, cap)
        place = (spot == slot(gcol, rank_col)).astype(jnp.bfloat16)
        out_ref[...] = jnp.dot(
            place, back[...].reshape(ranks * slots, cols), preferred_element_type=jnp.float32
        ).astype(jnp.bfloat16)
        for sem, size in pending.values():
            wait_of(bulk(size), sem).wait_send()


def solution(mesh):
    ep_count, tp_count = mesh.shape["ep"], mesh.shape["tp"]

    def on_device(
        hidden_in, norm_gain, group_ids, inner_ids, group_prob, expert_prob, w_gate, w_up, w_down
    ):
        tokens = hidden_in.shape[0]
        experts, depth, hidden = w_gate.shape
        cols = w_down.shape[2]
        ranks, cap = EPG // experts, tokens // 2
        groups, ys = ep_count // ranks, tp_count // CORES
        feats, side = depth // tp_count, depth // CORES
        others = max(groups - 1, 1)
        hbm = pl.BlockSpec(memory_space=pl.ANY)
        dma = pltpu.SemaphoreType.DMA
        small = (
            hidden_in, norm_gain.reshape(1, depth), group_ids.reshape(1, tokens), inner_ids.T,
            group_prob.reshape(1, tokens), expert_prob.T,
        )
        return pl.pallas_call(
            functools.partial(moe_kernel, ep_count, tp_count),
            out_shape=pltpu.VMEM((tokens, cols), jnp.bfloat16),
            in_specs=[hbm] * 9,
            out_specs=pl.BlockSpec(memory_space=pltpu.VMEM),
            scratch_shapes=[pltpu.VMEM(a.shape, a.dtype) for a in small] + [
                pltpu.VMEM(w_gate.shape, jnp.bfloat16),
                pltpu.VMEM(w_up.shape, jnp.bfloat16),
                pltpu.VMEM(w_down.shape, jnp.bfloat16),
                pltpu.VMEM((others, cap, feats + LANES), jnp.bfloat16),
                pltpu.VMEM((CORES, ranks * cap, side + LANES), jnp.bfloat16),
                pltpu.VMEM((groups, CORES, ys, ranks * cap, feats + LANES), jnp.bfloat16),
                pltpu.VMEM((groups, CORES, ys, ranks * cap, experts * hidden), jnp.bfloat16),
                pltpu.VMEM((groups, ranks * cap, cols), jnp.bfloat16),
                pltpu.VMEM((groups, ranks, cap, cols), jnp.bfloat16),
                dma((len(small),)), dma((3,)), dma((groups,)),
                dma((others,)), dma((ranks - 1,)), dma((1,)),
                dma((others, ranks * ys - 1)), dma((others, ys + 1)),
                dma((groups, CHUNKS, ys - 1)), dma((groups, CHUNKS, ys)), dma((groups,)),
            ],
            compiler_params=pltpu.CompilerParams(
                collective_id=0, has_side_effects=True, vmem_limit_bytes=56 * 1024 * 1024
            ),
        )(*small, w_gate, w_up, w_down)

    placed = (
        P("ep", None), P(), P("ep"), P("ep", None), P("ep"), P("ep", None),
        P("ep", None, "tp"), P("ep", None, "tp"), P("ep", None, "tp"),
    )
    return jax.shard_map(
        on_device, mesh=mesh, in_specs=placed, out_specs=P("ep", "tp"), check_vma=False
    )
```

profile of v0, /device:TPU:0, one launch (start us, length us, event | category | flops | bytes accessed | tf_op | source)
XLA Modules:
  0.0 26.6 jit_solution(8237192896302790582)
XLA Ops:
  0.0 26.0 %shard_map.91 = bf16[32,1024]{1,0:T(8,128)(2,1)S(1)} custom-call(bf16[32,4096]{1,0:T(8,128)(2,1)} %hid_hbm.1, f32[1,4096]{1,0:T(1,128)} %bitcast.5, s32[1,32]{1,0:T(1,128)} %bitcast.8, s32[4,32]{1,0:T(4,128)} %bitcast.6, f32[1,32]{1,0:T(1,128)} %bitcast.9, f32[4,32]{1,0:T(4,128)} %bitcast.7, bf16[2,4096,256]{2,1,0:T(8,128)(2,1)} %wg_hbm.1, ...), custom_call_target="tpu_custom_call" | custom-call | tf_op jit(solution)/shard_map/pallas_call | solution.py:386
  26.0 0.6 %copy.11 = bf16[32,1024]{1,0:T(8,128)(2,1)} copy(bf16[32,1024]{1,0:T(8,128)(2,1)S(1)} %shard_map.91) | data formatting | bytes 131072
where the time goes:
time: 26.8 us; the launch traced here: 26.6 us
  Pallas kernels  26 us (97%)
  local copies, waits for them, and re-layouts  0.63 us (2%)
    pallas_call x1, Pallas kernels, on_device(): pl.pallas_call(functools.partial(moe_kernel, ep_count, tp_count), out_sha...  26 us
    unnamed x1, local copies, waits for them, and re-layouts  0.63 us

commit v1 on v0

--- a/solution.py
+++ b/solution.py
@@ -25,7 +25,7 @@
     out_ref,
     hid_ref, gain_ref, grp_ref, inner_ref, gprob_ref, eprob_ref,
     wg, wu, wd, rows_out, rows_own, rows_in, acts, parts, back,
-    i_sem, w_sem, step_send, a_recv, s_recv, q_recv, b_recv, r_recv, h_recv, hr_recv, o_recv,
+    i_sem, w_sem, step_send, a_recv, s_recv, q_recv, b_recv, r_recv, h_recv, hr_recv, g_recv, o_recv,
 ):
     experts, depth, hidden = wg.shape
     ranks = EPG // experts
@@ -71,6 +71,9 @@
         for dy in range(ys):
             greet(g * ranks + to(d), twin(dy))
             partners += 1
+    for dy in range(1, ys):
+        greet(me_ep, lax.rem(y + dy, ys) * CORES + c)
+        partners += 1
 
     fetched = []
     for k, (src, dst) in enumerate((
@@ -239,7 +242,12 @@
                     acts[j, c, y, rows, e * hidden : (e + 1) * hidden] = act.astype(jnp.bfloat16)
                 held = acts.at[j, c, y, rows]
                 for dy in range(1, ys):
-                    send(held, held, step_send.at[j], h_recv.at[j, k, dy - 1], me_ep, twin(dy), j)
+                    if j == 0:
+                        send(held, held, step_send.at[j], h_recv.at[dy - 1], me_ep, twin(dy), j)
+                        continue
+                    for core in reversed(range(CORES)):
+                        send(held, held, step_send.at[j], g_recv.at[j - 1, k, c, dy - 1], me_ep,
+                             lax.rem(y + dy, ys) * CORES + core, j)
                 send(held, held, step_send.at[j], hr_recv.at[j, k, 0], me_ep, twin(), j)
 
         if j == 0:
@@ -300,24 +308,21 @@
             landed(acts.at[j, sib, y, cuts[k]], hr_recv.at[j, k, 0])
         whole = multiply(sib, 0, slice(None), whole)
 
-        def relay(k):
+        if j == 0:
             for dy in range(1, ys):
-                got = acts.at[j, sib, rem(y - dy, ys), cuts[k]]
-                landed(got, h_recv.at[j, k, dy - 1])
-                send(got, got, step_send.at[j], hr_recv.at[j, k, dy], me_ep, twin(), j)
-
-        relay(0)
+                got = acts.at[0, sib, rem(y - dy, ys)]
+                landed(got, h_recv.at[dy - 1])
+                send(got, got, step_send.at[0], hr_recv.at[0, 0, dy], me_ep, twin(), 0)
         for k, rows in enumerate(cuts):
-            if k:
-                collect(j - 1)
             total = whole[rows]
             for dy in range(1, ys):
-                total = multiply(sib, dy, rows, total)
-            if k + 1 < len(cuts):
-                relay(k + 1)
-            for dy in range(1, ys):
-                landed(acts.at[j, c, rem(y - dy, ys), rows], hr_recv.at[j, k, dy])
-                total = multiply(c, dy, rows, total)
+                for core in (sib, c):
+                    got = acts.at[j, core, rem(y - dy, ys), rows]
+                    if j:
+                        landed(got, g_recv.at[j - 1, k, core, dy - 1])
+                    elif core is c:
+                        landed(got, hr_recv.at[0, 0, dy])
+                    total = multiply(core, dy, rows, total)
             parts[j, rows] = total.astype(jnp.bfloat16)
             if j == 0:
                 for d in near:
@@ -325,6 +330,8 @@
                          g * ranks + to(d), me_tp, 0)
                 back[0, p] = parts[0, lines(p), :]
                 continue
+            if k:
+                collect(j - 1)
             for r in range(rows.start // cap, rows.stop // cap):
                 send(parts.at[j, lines(r)], back.at[j, p], step_send.at[j], o_recv.at[j],
                      lax.rem(g + j, groups) * ranks + r, me_tp, j)
@@ -401,7 +408,8 @@
                 dma((len(small),)), dma((3,)), dma((groups,)),
                 dma((others,)), dma((ranks - 1,)), dma((1,)),
                 dma((others, ranks * ys - 1)), dma((others, ys + 1)),
-                dma((groups, CHUNKS, ys - 1)), dma((groups, CHUNKS, ys)), dma((groups,)),
+                dma((ys - 1,)), dma((groups, CHUNKS, ys)),
+                dma((others, CHUNKS, CORES, ys - 1)), dma((groups,)),
             ],
             compiler_params=pltpu.CompilerParams(
                 collective_id=0, has_side_effects=True, vmem_limit_bytes=56 * 1024 * 1024

time: 26.8 us -> 26.5 us (0.989)
  the two profiles are of different devices: /device:TPU:0 before, /device:TPU:10 now
where the time goes in v1:
time: 26.5 us; the launch traced here: 26.4 us
  Pallas kernels  25.7 us (97%)
  local copies, waits for them, and re-layouts  0.63 us (2%)
    pallas_call x1, Pallas kernels, on_device(): pl.pallas_call(functools.partial(moe_kernel, ep_count, tp_count), out_sha...  25.7 us
    unnamed x1, local copies, waits for them, and re-layouts  0.63 us

profile of v1, /device:TPU:10, one launch (start us, length us, event | category | flops | bytes accessed | tf_op | source)
XLA Modules:
  0.0 26.4 jit_solution(12819264939291861065)
XLA Ops:
  0.0 25.7 %shard_map.91 = bf16[32,1024]{1,0:T(8,128)(2,1)S(1)} custom-call(bf16[32,4096]{1,0:T(8,128)(2,1)} %hid_hbm.1, f32[1,4096]{1,0:T(1,128)} %bitcast.5, s32[1,32]{1,0:T(1,128)} %bitcast.8, s32[4,32]{1,0:T(4,128)} %bitcast.6, f32[1,32]{1,0:T(1,128)} %bitcast.9, f32[4,32]{1,0:T(4,128)} %bitcast.7, bf16[2,4096,256]{2,1,0:T(8,128)(2,1)} %wg_hbm.1, ...), custom_call_target="tpu_custom_call" | custom-call | tf_op jit(solution)/shard_map/pallas_call | solution.py:393
  25.7 0.6 %copy.11 = bf16[32,1024]{1,0:T(8,128)(2,1)} copy(bf16[32,1024]{1,0:T(8,128)(2,1)S(1)} %shard_map.91) | data formatting | bytes 131072
